TPU v7x, 32 devices: a whole 2x2x4 slice. The times are simulated.
32 devices in a mesh: sp: 8 (over z, y), tp: 4 (over x, core).
Axes of the slice: x: 2, y: 2, z: 4, core: 2. Of those that a mesh axis runs over, the one named last changes fastest.
Arguments:
- query_first: bfloat16 [6144, 8, 128], P('sp', 'tp'), may hold values from -5.375 to 5.375
- key_first: bfloat16 [6144, 8, 128], P('sp', 'tp'), may hold values from -5.375 to 5.375
- value_first: bfloat16 [6144, 8, 128], P('sp', 'tp'), may hold values from -6 to 6
- query_second: bfloat16 [6144, 8, 256], P('sp', 'tp'), may hold values from -5.375 to 5.375
- key_second: bfloat16 [6144, 8, 256], P('sp', 'tp'), may hold values from -5.375 to 5.375
- value_second: bfloat16 [6144, 8, 128], P('sp', 'tp'), may hold values from -6 to 6
- mix_lambda: float32 [2, 8], P(None, 'tp'), may hold values from 0.3 to 0.8
- head_gain: float32 [2, 8, 128], P(None, 'tp'), may hold values from 0.1 to 1.9
- out_weight: bfloat16 [2, 8, 128, 2048], P(None, 'tp'), may hold values from -0.125 to 0.125
- residual: bfloat16 [6144, 2048], P(('sp', 'tp')), may hold values from -6 to 6
- norm_gain: float32 [2, 2048], replicated, may hold values from 0.1 to 1.9
- up_weight: bfloat16 [2048, 8192], P('sp', 'tp'), may hold values from -0.125 to 0.125
- down_weight: bfloat16 [8192, 2048], P('tp', 'sp'), may hold values from -0.0625 to 0.0625
Outputs:
- mixed: bfloat16 [6144, 2048], P(('sp', 'tp'))
All inputs are finite; a program needn't handle non-finite values.
Results may differ from a plain program's by a relative error of at most 0.02.
Values may be sent and summed in bfloat16 or wider, within the bound.
A program may use at most 128 MiB of HBM per device.

v0:
```python
import math
import jax
import jax.numpy as jnp
from jax import lax
from jax.sharding import PartitionSpec as P

EPSILON = 1e-05
LOWEST = -1e30


def layer_norm(activations, scales):
    average = jnp.mean(activations, axis=-1, keepdims=True)
    centred = activations - average
    spread = jnp.mean(centred * centred, axis=-1, keepdims=True)
    return centred * lax.rsqrt(spread + EPSILON) * scales


def fold_group(carried, queries, key_rows, values, score_scale):
    maxima, totals, numerator = carried
    scores = (
        jnp.einsum("qhck,phck->hcqp", queries, key_rows, preferred_element_type=jnp.float32)
        * score_scale
    )
    newest = jnp.maximum(maxima, jnp.max(scores, axis=-1))
    weights = jnp.exp(scores - newest[..., None])
    factor = jnp.exp(maxima - newest)
    totals = totals * factor + jnp.sum(weights, axis=-1)
    numerator = numerator * factor[..., None] + jnp.einsum(
        "hcqp,phv->hcqv", weights.astype(jnp.bfloat16), values, preferred_element_type=jnp.float32
    )
    return (newest, totals, numerator)


def finish_group(carried, lambdas, gains):
    maxima, totals, numerator = carried
    attended = (
        numerator[:, 0] / totals[:, 0, :, None]
        - lambdas[:, None, None] * numerator[:, 1] / totals[:, 1, :, None]
    )
    mean_square = jnp.mean(attended * attended, axis=-1, keepdims=True)
    return (attended * lax.rsqrt(mean_square + EPSILON) * gains[:, None, :]).astype(jnp.bfloat16)


def squared_relu(expanded):
    return jnp.square(jnp.maximum(expanded, 0.0)).astype(jnp.bfloat16)


def local(
    query_first,
    key_first,
    value_first,
    query_second,
    key_second,
    value_second,
    mix_lambda,
    head_gain,
    out_weight,
    residual,
    norm_gain,
    up_weight,
    down_weight,
):
    up_whole, down_whole = (
        lax.all_gather(up_weight, "sp", axis=0, tiled=True),
        lax.all_gather(down_weight, "sp", axis=1, tiled=True),
    )
    tok_dev, local_heads, width_first = query_first.shape
    size_first = width_first // 2
    size_second = query_second.shape[2] // 2
    value_size = value_first.shape[2]
    scale_first = 1.0 / math.sqrt(size_first)
    scale_second = 1.0 / math.sqrt(size_second)
    queries_first = query_first.reshape(tok_dev, local_heads, 2, size_first)
    queries_second = query_second.reshape(tok_dev, local_heads, 2, size_second)

    def initial():
        return (
            jnp.full((local_heads, 2, tok_dev), LOWEST, jnp.float32),
            jnp.zeros((local_heads, 2, tok_dev), jnp.float32),
            jnp.zeros((local_heads, 2, tok_dev, value_size), jnp.float32),
        )

    carried = (initial(), initial())
    pieces = (
        lax.all_gather(key_first, "sp", axis=0, tiled=True),
        lax.all_gather(key_second, "sp", axis=0, tiled=True),
        lax.all_gather(value_first, "sp", axis=0, tiled=True),
        lax.all_gather(value_second, "sp", axis=0, tiled=True),
    )
    length = pieces[0].shape[0]
    block_count = length // tok_dev
    segments = tuple(
        (member.reshape((block_count, tok_dev) + member.shape[1:]) for member in pieces)
    )

    def absorb_block(running, segment):
        keys_one, keys_two, values_one, values_two = segment
        first_state = fold_group(
            running[0],
            queries_first,
            keys_one.reshape(tok_dev, local_heads, 2, size_first),
            values_one,
            scale_first,
        )
        second_state = fold_group(
            running[1],
            queries_second,
            keys_two.reshape(tok_dev, local_heads, 2, size_second),
            values_two,
            scale_second,
        )
        return ((first_state, second_state), None)

    carried, unused = lax.scan(absorb_block, carried, segments)
    state_first, state_second = carried
    heads_first = finish_group(state_first, mix_lambda[0], head_gain[0])
    heads_second = finish_group(state_second, mix_lambda[1], head_gain[1])
    stacked = jnp.stack([heads_first, heads_second])
    selected = stacked
    projected = lax.psum_scatter(
        jnp.einsum(
            "ghqv,ghvd->qd", selected, out_weight, preferred_element_type=jnp.float32
        ).astype(jnp.bfloat16),
        "tp",
        scatter_dimension=0,
        tiled=True,
    ).astype(jnp.float32) + residual.astype(jnp.float32)
    normed = layer_norm(projected, norm_gain[0])
    mixer_in = lax.all_gather(normed.astype(jnp.bfloat16), "tp", axis=0, tiled=True)
    hidden = squared_relu(jnp.dot(mixer_in, up_whole, preferred_element_type=jnp.float32))
    selected = hidden
    mixed_sum = lax.psum_scatter(
        jnp.dot(selected, down_whole, preferred_element_type=jnp.float32).astype(jnp.bfloat16),
        "tp",
        scatter_dimension=0,
        tiled=True,
    ).astype(jnp.float32)
    return layer_norm(normed + mixed_sum, norm_gain[1]).astype(jnp.bfloat16)


def solution(mesh):
    return jax.shard_map(
        local,
        mesh=mesh,
        in_specs=(
            P("sp", "tp", None),
            P("sp", "tp", None),
            P("sp", "tp", None),
            P("sp", "tp", None),
            P("sp", "tp", None),
            P("sp", "tp", None),
            P(None, "tp"),
            P(None, "tp", None),
            P(None, "tp", None, None),
            P(("sp", "tp"), None),
            P(),
            P("sp", "tp"),
            P("tp", "sp"),
        ),
        out_specs=P(("sp", "tp"), None),
        check_vma=False,
    )
```

profile of v0, /device:TPU:0, one launch (start us, length us, event | category | flops | bytes accessed | tf_op | source)
XLA Modules:
  0.0 893.3 jit_solution(1156918713239734366)
XLA Ops:
  18.3 54.0 %all-gather.8.cloned.1.call-done = bf16[6144,2,128]{2,0,1:T(8,128)(2,1)} async-done(((bf16[768,2,128]{2,0,1:T(8,128)(2,1)}), bf16[6144,2,128]{2,0,1:T(8,128)(2,1)}) %all-gather.8.cloned.1.call-update) | async-done | bytes 3145744 | tf_op jit(solution)/shard_map/all_gather | solution.py:85
  72.3 60.9 %all-gather.10.cloned.1.call-done = bf16[6144,2,128]{2,0,1:T(8,128)(2,1)} async-done(((bf16[768,2,128]{2,0,1:T(8,128)(2,1)}), bf16[6144,2,128]{2,0,1:T(8,128)(2,1)}) %all-gather.10.cloned.1.call-update) | async-done | bytes 3145744 | tf_op jit(solution)/shard_map/all_gather | solution.py:87
  133.2 60.9 %all-gather.14.cloned.1.call-done = bf16[6144,2,128]{2,0,1:T(8,128)(2,1)} async-done(((bf16[768,2,128]{2,0,1:T(8,128)(2,1)}), bf16[6144,2,128]{2,0,1:T(8,128)(2,1)}) %all-gather.14.cloned.1.call-update) | async-done | bytes 3145744 | tf_op jit(solution)/shard_map/all_gather | solution.py:88
  194.1 99.4 %all-gather.12.cloned.1.call-done = bf16[6144,2,256]{2,0,1:T(8,128)(2,1)} async-done(((bf16[768,2,256]{2,0,1:T(8,128)(2,1)}), bf16[6144,2,256]{2,0,1:T(8,128)(2,1)}) %all-gather.12.cloned.1.call-update) | async-done | bytes 6291472 | tf_op jit(solution)/shard_map/all_gather | solution.py:86
  293.6 214.6 %while.21 = (s32[]{:T(128)}, f32[2,2,768]{2,1,0:T(2,128)S(1)}, f32[2,2,768]{2,1,0:T(2,128)}, f32[2,2,768,128]{3,2,1,0:T(8,128)}, f32[2,2,768]{2,1,0:T(2,128)S(1)...) while((s32[]{:T(128)}, f32[2,2,768]{2,1,0:T(2,128)S(1)}, ...), condition=%wide.region_5.6_spmd.clone, body=%wide.region_0.5_spmd.clone.sunk | while | flops 2154067968 | bytes 149816656 | solution.py:114
  309.2 4.8 fusion.103
  314.0 3.8 fusion.102
  329.8 2.6 bitcast_reduce_fusion.5
  336.1 4.9 fusion.103
  341.0 3.8 fusion.102
  356.8 2.6 bitcast_reduce_fusion.5
  363.1 4.9 fusion.103
  368.1 3.8 fusion.102
  390.2 4.9 fusion.103
  395.1 3.8 fusion.102
  410.9 2.6 bitcast_reduce_fusion.5
  417.2 4.9 fusion.103
  422.1 3.8 fusion.102
  444.2 4.9 fusion.103
  449.1 3.8 fusion.102
  471.2 4.9 fusion.103
  476.2 3.8 fusion.102
  498.3 4.9 fusion.103
  503.2 3.8 fusion.102
  514.0 3.2 bitcast_convert_fusion
  517.9 35.5 %reduce-scatter.3.cloned.1.call-done = bf16[192,2048]{1,0:T(8,128)(2,1)} async-done(((bf16[768,2048]{1,0:T(8,128)(2,1)}), bf16[192,2048]{1,0:T(8,128)(2,1)}) %reduce-scatter.3.cloned.1.call-update) | async-done | bytes 786448 | tf_op jit(solution)/shard_map/reduce_scatter | solution.py:120
  557.4 122.5 %all-gather.18.cloned.1.call-done = bf16[2048,2048]{1,0:T(8,128)(2,1)} async-done(((bf16[256,2048]{1,0:T(8,128)(2,1)}), bf16[2048,2048]{1,0:T(8,128)(2,1)}) %all-gather.18.cloned.1.call-update) | async-done | bytes 8388624 | tf_op jit(solution)/shard_map/all_gather | solution.py:64
  679.9 28.3 %all-gather.16.cloned.1.call-done = bf16[768,2048]{1,0:T(8,128)(2,1)} async-done(((bf16[192,2048]{1,0:T(8,128)(2,1)}), bf16[768,2048]{1,0:T(8,128)(2,1)}) %all-gather.16.cloned.1.call-update) | async-done | bytes 3145744 | tf_op jit(solution)/shard_map/all_gather | solution.py:129
  708.2 11.9 %multiply_convert_fusion = bf16[768,2048]{1,0:T(8,128)(2,1)} fusion(bf16[768,2048]{1,0:T(8,128)(2,1)} %all-gather.16.cloned.1.call-done, bf16[2048,2048]{1,0:T(8,128)(2,1)} %all-gather.18.cloned.1.call-done), kind=kOutput, calls=%fused_computation.41 | convolution fusion | flops 6447169536 | bytes 14680064 | tf_op jit(solution)/shard_map/dot_general | solution.py:130
  720.0 115.2 %all-gather.20.cloned.1.call-done = bf16[2048,2048]{1,0:T(8,128)(2,1)} async-done(((bf16[2048,256]{1,0:T(8,128)(2,1)}), bf16[2048,2048]{1,0:T(8,128)(2,1)}) %all-gather.20.cloned.1.call-update) | async-done | bytes 8388624 | tf_op jit(solution)/shard_map/all_gather | solution.py:65
  835.2 11.8 %convolution_convert_fusion = bf16[768,2048]{1,0:T(8,128)(2,1)} fusion(bf16[768,2048]{1,0:T(8,128)(2,1)} %multiply_convert_fusion, bf16[2048,2048]{1,0:T(8,128)(2,1)} %all-gather.20.cloned.1.call-done), kind=kOutput, calls=%fused_computation.42 | convolution fusion | flops 6444023808 | bytes 14680064 | tf_op jit(solution)/shard_map/dot_general | solution.py:133
  847.1 36.2 %reduce-scatter.5.cloned.1.call-done = bf16[192,2048]{1,0:T(8,128)(2,1)} async-done(((bf16[768,2048]{1,0:T(8,128)(2,1)}), bf16[192,2048]{1,0:T(8,128)(2,1)}) %reduce-scatter.5.cloned.1.call-update) | async-done | bytes 786448 | tf_op jit(solution)/shard_map/reduce_scatter | solution.py:132
  (288 shorter events, 162.1 us)
Async XLA Ops:
  6.5 507.4 %copy-start = (bf16[2,2,128,2048]{3,2,1,0:T(8,128)(2,1)S(1)}, bf16[2,2,128,2048]{3,2,1,0:T(8,128)(2,1)}, u32[]{:S(2)}) copy-start(bf16[2,2,128,2048]{3,2,1,0:T(8,128)(2,1)} %param.23) | copy-start | bytes 6291460
  6.5 65.8 %all-gather.8.cloned.1.call-start = ((), (), s32[]{:S(2)}) async-start(), calls=%async_computation.2 | async-start | bytes 3538944 | tf_op jit(solution)/shard_map/all_gather | solution.py:85
  8.5 124.7 %all-gather.10.cloned.1.call-start = ((), (), s32[]{:S(2)}) async-start(), calls=%async_computation.3 | async-start | bytes 3538944 | tf_op jit(solution)/shard_map/all_gather | solution.py:87
  10.4 183.7 %all-gather.14.cloned.1.call-start = ((), (), s32[]{:S(2)}) async-start(), calls=%async_computation.5 | async-start | bytes 3538944 | tf_op jit(solution)/shard_map/all_gather | solution.py:88
  11.4 282.2 %all-gather.12.cloned.1.call-start = ((), (), s32[]{:S(2)}) async-start(), calls=%async_computation.4 | async-start | bytes 7077888 | tf_op jit(solution)/shard_map/all_gather | solution.py:86
  12.4 541.0 %reduce-scatter.3.cloned.1.call-start = ((), (), s32[]{:S(2)}) async-start(), calls=%async_computation.6 | async-start | bytes 3932160 | tf_op jit(solution)/shard_map/reduce_scatter | solution.py:120
  307.0 7.0 slice-start
  307.0 7.0 slice-start.1
  332.4 8.6 slice-start
  332.4 8.6 slice-start.1
  336.1 4.9 copy-start.2
  359.5 8.6 slice-start
  359.5 8.6 slice-start.1
  363.1 4.9 copy-start.2
  386.5 8.6 slice-start
  386.5 8.6 slice-start.1
  390.2 4.9 copy-start.2
  413.5 8.6 slice-start
  413.5 8.6 slice-start.1
  417.2 4.9 copy-start.2
  440.5 8.6 slice-start
  440.5 8.6 slice-start.1
  444.2 4.9 copy-start.2
  467.5 8.6 slice-start
  467.6 8.6 slice-start.1
  494.6 8.6 slice-start
  494.6 8.6 slice-start.1
  517.2 36.2 %copy-start.6 = (bf16[192,2048]{1,0:T(8,128)(2,1)S(1)}, bf16[192,2048]{1,0:T(8,128)(2,1)}, u32[]{:S(2)}) copy-start(bf16[192,2048]{1,0:T(8,128)(2,1)} %param.24) | copy-start | bytes 2359300
  517.2 162.7 %all-gather.18.cloned.1.call-start = ((), (), s32[]{:S(2)}) async-start(), calls=%async_computation.8 | async-start | bytes 9437184 | tf_op jit(solution)/shard_map/all_gather | solution.py:64
  517.8 190.4 %all-gather.16.cloned.1.call-start = ((), (), s32[]{:S(2)}) async-start(), calls=%async_computation.7 | async-start | bytes 3932160 | tf_op jit(solution)/shard_map/all_gather | solution.py:129
  556.6 278.6 %all-gather.20.cloned.1.call-start = ((), (), s32[]{:S(2)}) async-start(), calls=%async_computation.9 | async-start | bytes 9437184 | tf_op jit(solution)/shard_map/all_gather | solution.py:65
  557.4 325.9 %reduce-scatter.5.cloned.1.call-start = ((), (), s32[]{:S(2)}) async-start(), calls=%async_computation.10 | async-start | bytes 3932160 | tf_op jit(solution)/shard_map/reduce_scatter | solution.py:132
  (39 other events, 124.4 us)
Sparse Core Ops, SparseCore 0:
  9.5 62.7 all-gather.7
  74.5 58.6 all-gather.9
  135.4 58.6 all-gather.13
  196.2 97.3 all-gather.11
  517.3 36.0 reduce-scatter.2
  555.4 124.4 all-gather.17
  681.5 26.6 all-gather.15
  710.2 124.9 all-gather.19
  847.2 36.0 reduce-scatter.4
where the time goes:
time: 895 us; the launch traced here: 893 us
  waiting for transfers between devices  614 us (69%)
  matrix products  136 us (15%)
  local copies, waits for them, and re-layouts  76 us (8%)
  other arithmetic  52 us (6%)
  between operations  13.5 us (2%)
    all_gather x1, waiting for transfers between devices, local(): lax.all_gather(up_weight, 'sp', axis=0, tiled=True)  122 us
    all_gather x1, waiting for transfers between devices, local(): lax.all_gather(down_weight, 'sp', axis=1, tiled=True)  115 us
    all_gather x1, waiting for transfers between devices, local(): lax.all_gather(key_second, 'sp', axis=0, tiled=True)  99.4 us
    dot_general x16, matrix products, fold_group(): jnp.einsum('hcqp,phv->hcqv', weights.astype(jnp.bfloat16), values, prefer...  69.2 us
    all_gather x1, waiting for transfers between devices, local(): lax.all_gather(value_second, 'sp', axis=0, tiled=True)  60.9 us
    all_gather x1, waiting for transfers between devices, local(): lax.all_gather(value_first, 'sp', axis=0, tiled=True)  60.9 us
    all_gather x1, waiting for transfers between devices, local(): lax.all_gather(key_first, 'sp', axis=0, tiled=True)  54 us
    dot_general x16, matrix products, fold_group(): jnp.einsum('qhck,phck->hcqp', queries, key_rows, preferred_element_type=j...  40.3 us
  transfers between devices with their start and end apart: 9, of which 9 were waited for; matrix products, arithmetic and copies ran while one was open for 3% of the time, Pallas kernels for 0%

commit v1 on v0

--- a/solution.py
+++ b/solution.py
@@ -62,7 +62,7 @@
 ):
     up_whole, down_whole = (
         lax.all_gather(up_weight, "sp", axis=0, tiled=True),
-        lax.all_gather(down_weight, "sp", axis=1, tiled=True),
+        jnp.concatenate(lax.all_gather(down_weight, "sp"), axis=1),
     )
     tok_dev, local_heads, width_first = query_first.shape
     size_first = width_first // 2

time: 895 us -> 902 us (level)
  local copies, waits for them, and re-layouts: 76 us -> 87.8 us
    reshape x0 -> x1, local copies, waits for them, and re-layouts: none -> 11.7 us  [local(): jnp.concatenate(lax.all_gather(down_weight, 'sp'), axis=1)]
    all_gather x1, waiting for transfers between devices: 122 us -> 113 us  [local(): lax.all_gather(up_weight, 'sp', axis=0, tiled=True)]
where the time goes in v1:
time: 902 us; the launch traced here: 899 us
  waiting for transfers between devices  614 us (68%)
  matrix products  131 us (15%)
  local copies, waits for them, and re-layouts  87.8 us (10%)
  other arithmetic  52 us (6%)
  between operations  13.5 us (1%)
    all_gather x1, waiting for transfers between devices, local(): lax.all_gather(down_weight, 'sp')  123 us
    all_gather x1, waiting for transfers between devices, local(): lax.all_gather(up_weight, 'sp', axis=0, tiled=True)  113 us
    all_gather x1, waiting for transfers between devices, local(): lax.all_gather(key_second, 'sp', axis=0, tiled=True)  99.4 us
    dot_general x16, matrix products, fold_group(): jnp.einsum('hcqp,phv->hcqv', weights.astype(jnp.bfloat16), values, prefer...  69.1 us
    all_gather x1, waiting for transfers between devices, local(): lax.all_gather(value_second, 'sp', axis=0, tiled=True)  60.9 us
    all_gather x1, waiting for transfers between devices, local(): lax.all_gather(value_first, 'sp', axis=0, tiled=True)  60.9 us
    all_gather x1, waiting for transfers between devices, local(): lax.all_gather(key_first, 'sp', axis=0, tiled=True)  54 us
    dot_general x16, matrix products, fold_group(): jnp.einsum('qhck,phck->hcqp', queries, key_rows, preferred_element_type=j...  40.3 us
  transfers between devices with their start and end apart: 9, of which 9 were waited for; matrix products, arithmetic and copies ran while one was open for 3% of the time, Pallas kernels for 0%

profile of v1, /device:TPU:0, one launch (start us, length us, event | category | flops | bytes accessed | tf_op | source)
XLA Modules:
  0.0 899.3 jit_solution(6496615378212958664)
XLA Ops:
  18.3 54.0 %all-gather.9.cloned.1.call-done = bf16[6144,2,128]{2,0,1:T(8,128)(2,1)} async-done(((bf16[768,2,128]{2,0,1:T(8,128)(2,1)}), bf16[6144,2,128]{2,0,1:T(8,128)(2,1)}) %all-gather.9.cloned.1.call-update) | async-done | bytes 3145744 | tf_op jit(solution)/shard_map/all_gather | solution.py:85
  72.3 60.9 %all-gather.11.cloned.1.call-done = bf16[6144,2,128]{2,0,1:T(8,128)(2,1)} async-done(((bf16[768,2,128]{2,0,1:T(8,128)(2,1)}), bf16[6144,2,128]{2,0,1:T(8,128)(2,1)}) %all-gather.11.cloned.1.call-update) | async-done | bytes 3145744 | tf_op jit(solution)/shard_map/all_gather | solution.py:87
  133.2 60.9 %all-gather.15.cloned.1.call-done = bf16[6144,2,128]{2,0,1:T(8,128)(2,1)} async-done(((bf16[768,2,128]{2,0,1:T(8,128)(2,1)}), bf16[6144,2,128]{2,0,1:T(8,128)(2,1)}) %all-gather.15.cloned.1.call-update) | async-done | bytes 3145744 | tf_op jit(solution)/shard_map/all_gather | solution.py:88
  194.1 99.4 %all-gather.13.cloned.1.call-done = bf16[6144,2,256]{2,0,1:T(8,128)(2,1)} async-done(((bf16[768,2,256]{2,0,1:T(8,128)(2,1)}), bf16[6144,2,256]{2,0,1:T(8,128)(2,1)}) %all-gather.13.cloned.1.call-update) | async-done | bytes 6291472 | tf_op jit(solution)/shard_map/all_gather | solution.py:86
  293.6 214.6 %while.21 = (s32[]{:T(128)}, f32[2,2,768]{2,1,0:T(2,128)S(1)}, f32[2,2,768]{2,1,0:T(2,128)}, f32[2,2,768,128]{3,2,1,0:T(8,128)}, f32[2,2,768]{2,1,0:T(2,128)S(1)...) while((s32[]{:T(128)}, f32[2,2,768]{2,1,0:T(2,128)S(1)}, ...), condition=%wide.region_5.6_spmd.clone, body=%wide.region_0.5_spmd.clone.sunk | while | flops 2154067968 | bytes 149816656 | solution.py:114
  309.2 4.7 fusion.103
  314.0 3.8 fusion.102
  336.1 4.9 fusion.103
  341.0 3.8 fusion.102
  363.2 4.9 fusion.103
  368.1 3.8 fusion.102
  383.9 2.6 bitcast_reduce_fusion.5
  390.2 4.9 fusion.103
  395.1 3.8 fusion.102
  417.2 4.9 fusion.103
  422.1 3.8 fusion.102
  444.2 4.9 fusion.103
  449.1 3.8 fusion.102
  465.0 2.6 bitcast_reduce_fusion.5
  471.3 4.9 fusion.103
  476.2 3.8 fusion.102
  498.3 4.9 fusion.103
  503.2 3.8 fusion.102
  514.0 3.2 bitcast_convert_fusion
  518.6 34.8 %reduce-scatter.3.cloned.1.call-done = bf16[192,2048]{1,0:T(8,128)(2,1)} async-done(((bf16[768,2048]{1,0:T(8,128)(2,1)}), bf16[192,2048]{1,0:T(8,128)(2,1)}) %reduce-scatter.3.cloned.1.call-update) | async-done | bytes 786448 | tf_op jit(solution)/shard_map/reduce_scatter | solution.py:120
  556.7 123.2 %all-gather.21.cloned.1.call-done = bf16[16384,256]{1,0:T(8,128)(2,1)} async-done(((bf16[2048,256]{1,0:T(8,128)(2,1)}), bf16[16384,256]{1,0:T(8,128)(2,1)}) %all-gather.21.cloned.1.call-update) | async-done | bytes 8388624 | tf_op jit(solution)/shard_map/all_gather | solution.py:65
  679.9 11.7 %copy.55 = bf16[2048,8,256]{0,2,1:T(8,128)(2,1)} copy(bf16[2048,8,256]{2,0,1:T(8,128)(2,1)} %bitcast.187) | data formatting | bytes 16777216 | tf_op jit(solution)/shard_map/reshape | solution.py:65
  691.6 113.1 %all-gather.19.cloned.1.call-done = bf16[2048,2048]{1,0:T(8,128)(2,1)} async-done(((bf16[256,2048]{1,0:T(8,128)(2,1)}), bf16[2048,2048]{1,0:T(8,128)(2,1)}) %all-gather.19.cloned.1.call-update) | async-done | bytes 8388624 | tf_op jit(solution)/shard_map/all_gather | solution.py:64
  804.7 28.3 %all-gather.17.cloned.1.call-done = bf16[768,2048]{1,0:T(8,128)(2,1)} async-done(((bf16[192,2048]{1,0:T(8,128)(2,1)}), bf16[768,2048]{1,0:T(8,128)(2,1)}) %all-gather.17.cloned.1.call-update) | async-done | bytes 3145744 | tf_op jit(solution)/shard_map/all_gather | solution.py:129
  833.0 10.2 %multiply_convert_fusion = bf16[768,2048]{1,0:T(8,128)(2,1)S(1)} fusion(bf16[768,2048]{1,0:T(8,128)(2,1)} %all-gather.17.cloned.1.call-done, bf16[2048,2048]{1,0:T(8,128)(2,1)} %all-gather.19.cloned.1.call-done), kind=kOutput, calls=%fused_computation.41 | convolution fusion | flops 6447169536 | bytes 14680064 | tf_op jit(solution)/shard_map/dot_general | solution.py:130
  843.2 8.1 convolution_convert_fusion
  851.3 38.0 %reduce-scatter.5.cloned.1.call-done = bf16[192,2048]{1,0:T(8,128)(2,1)} async-done(((bf16[768,2048]{1,0:T(8,128)(2,1)}), bf16[192,2048]{1,0:T(8,128)(2,1)}) %reduce-scatter.5.cloned.1.call-update) | async-done | bytes 786448 | tf_op jit(solution)/shard_map/reduce_scatter | solution.py:132
  (291 shorter events, 164.8 us)
Async XLA Ops:
  6.5 507.5 %copy-start = (bf16[2,2,128,2048]{3,2,1,0:T(8,128)(2,1)S(1)}, bf16[2,2,128,2048]{3,2,1,0:T(8,128)(2,1)}, u32[]{:S(2)}) copy-start(bf16[2,2,128,2048]{3,2,1,0:T(8,128)(2,1)} %param.23) | copy-start | bytes 6291460
  6.5 65.8 %all-gather.9.cloned.1.call-start = ((), (), s32[]{:S(2)}) async-start(), calls=%async_computation.2 | async-start | bytes 3538944 | tf_op jit(solution)/shard_map/all_gather | solution.py:85
  8.5 124.7 %all-gather.11.cloned.1.call-start = ((), (), s32[]{:S(2)}) async-start(), calls=%async_computation.3 | async-start | bytes 3538944 | tf_op jit(solution)/shard_map/all_gather | solution.py:87
  10.4 183.7 %all-gather.15.cloned.1.call-start = ((), (), s32[]{:S(2)}) async-start(), calls=%async_computation.5 | async-start | bytes 3538944 | tf_op jit(solution)/shard_map/all_gather | solution.py:88
  11.3 282.2 %all-gather.13.cloned.1.call-start = ((), (), s32[]{:S(2)}) async-start(), calls=%async_computation.4 | async-start | bytes 7077888 | tf_op jit(solution)/shard_map/all_gather | solution.py:86
  12.4 541.0 %reduce-scatter.3.cloned.1.call-start = ((), (), s32[]{:S(2)}) async-start(), calls=%async_computation.6 | async-start | bytes 3932160 | tf_op jit(solution)/shard_map/reduce_scatter | solution.py:120
  307.0 7.0 slice-start
  307.0 7.0 slice-start.1
  332.5 8.6 slice-start
  332.5 8.6 slice-start.1
  336.1 4.9 copy-start.2
  359.5 8.6 slice-start
  359.5 8.6 slice-start.1
  363.2 4.9 copy-start.2
  386.5 8.6 slice-start
  386.5 8.6 slice-start.1
  390.2 4.9 copy-start.2
  413.5 8.6 slice-start
  413.5 8.6 slice-start.1
  417.2 4.9 copy-start.2
  440.6 8.6 slice-start
  440.6 8.6 slice-start.1
  467.6 8.6 slice-start
  467.6 8.6 slice-start.1
  494.6 8.6 slice-start
  494.6 8.6 slice-start.1
  517.2 36.2 %copy-start.6 = (bf16[192,2048]{1,0:T(8,128)(2,1)S(1)}, bf16[192,2048]{1,0:T(8,128)(2,1)}, u32[]{:S(2)}) copy-start(bf16[192,2048]{1,0:T(8,128)(2,1)} %param.24) | copy-start | bytes 2359300
  517.2 162.7 %all-gather.21.cloned.1.call-start = ((), (), s32[]{:S(2)}) async-start(), calls=%async_computation.10 | async-start | bytes 9437184 | tf_op jit(solution)/shard_map/all_gather | solution.py:65
  517.8 286.9 %all-gather.19.cloned.1.call-start = ((), (), s32[]{:S(2)}) async-start(), calls=%async_computation.8 | async-start | bytes 9437184 | tf_op jit(solution)/shard_map/all_gather | solution.py:64
  518.6 314.4 %all-gather.17.cloned.1.call-start = ((), (), s32[]{:S(2)}) async-start(), calls=%async_computation.7 | async-start | bytes 3932160 | tf_op jit(solution)/shard_map/all_gather | solution.py:129
  556.6 332.7 %reduce-scatter.5.cloned.1.call-start = ((), (), s32[]{:S(2)}) async-start(), calls=%async_computation.9 | async-start | bytes 3932160 | tf_op jit(solution)/shard_map/reduce_scatter | solution.py:132
  833.0 10.2 %copy-start.8 = (bf16[2048,8,256]{0,2,1:T(8,128)(2,1)S(1)}, bf16[2048,8,256]{0,2,1:T(8,128)(2,1)}, u32[]{:S(2)}) copy-start(bf16[2048,8,256]{0,2,1:T(8,128)(2,1)} %copy.55) | copy-start | bytes 25165828
  (40 other events, 130.1 us)
Sparse Core Ops, SparseCore 0:
  9.5 62.7 all-gather.8
  74.5 58.6 all-gather.10
  135.4 58.6 all-gather.14
  196.2 97.3 all-gather.12
  517.3 36.0 reduce-scatter.2
  555.4 124.4 all-gather.20
  682.0 122.6 all-gather.18
  806.3 26.6 all-gather.16
  851.4 37.8 reduce-scatter.4
